TPU v7x, 32 devices: a whole 2x2x4 slice. The times are simulated.
32 devices in a mesh: kv: 8 (over z, y), tp: 4 (over x, core).
Axes of the slice: x: 2, y: 2, z: 4, core: 2. Of those that a mesh axis runs over, the one named last changes fastest.
Arguments:
- tokens: bfloat16 [160, 4096], P(None, 'kv'), may hold values from -40 to 40
- input_norm_gain: float32 [4096], P('kv'), may hold values from 0.1 to 1.9
- input_matrix: bfloat16 [4096, 4096], P('kv', 'tp'), may hold values from -0.09375 to 0.09375
- gate_matrix: bfloat16 [4096, 4096], P('kv', 'tp'), may hold values from -0.09375 to 0.09375
- write_matrix: bfloat16 [4096, 1024], P('kv', 'tp'), may hold values from -0.09375 to 0.09375
- read_matrix: bfloat16 [4096, 1024], P('kv', 'tp'), may hold values from -0.09375 to 0.09375
- step_matrix: bfloat16 [4096, 64], replicated, may hold values from -0.09375 to 0.09375
- input_kernel: float32 [4, 4096], P(None, 'tp'), may hold values from -3 to 3
- write_kernel: float32 [4, 1024], P(None, 'tp'), may hold values from -3 to 3
- read_kernel: float32 [4, 1024], P(None, 'tp'), may hold values from -3 to 3
- step_size_bias: float32 [64], P('tp'), may hold values from -6 to 1
- head_decay_logs: float32 [64], P('tp'), may hold values from 0 to 2.77
- bypass_scale: float32 [64], P('tp'), may hold values from 0.5 to 1.5
- extra_decay_logs: float32 [160, 64], P('kv', 'tp'), may hold values from -0.7 to 0, as said below
- output_norm_gain: float32 [4096], P('tp'), may hold values from 0.1 to 1.9
- output_matrix: bfloat16 [4096, 4096], P('tp', 'kv'), may hold values from -0.09375 to 0.09375
- cached_state_history: float32 [32, 6, 64, 64, 128], P('kv', None, 'tp'), may hold values from -2 to 2
- cached_input_rows: bfloat16 [32, 8, 4096], P('kv', None, 'tp'), may hold values from -6 to 6
- cached_write_rows: bfloat16 [32, 8, 1024], P('kv', None, 'tp'), may hold values from -6 to 6
- cached_read_rows: bfloat16 [32, 8, 1024], P('kv', None, 'tp'), may hold values from -6 to 6
- accepted: int32 [32], P('kv'), may hold values from 0 to 5
Outputs:
- mixer_out: bfloat16 [160, 4096], P('tp', 'kv')
- next_states: float32 [32, 6, 64, 64, 128], P('kv', None, 'tp')
- next_input: bfloat16 [32, 8, 4096], P('kv', None, 'tp')
- next_write: bfloat16 [32, 8, 1024], P('kv', None, 'tp')
- next_read: bfloat16 [32, 8, 1024], P('kv', None, 'tp')
Inputs may be any that keep to these rules, and one draw needn't show every extreme that they name: `extra_decay_logs`: zero at most tokens and heads.
All inputs are finite; a program needn't handle non-finite values.
Results may differ from a plain program's by a relative error of at most 0.03.
Values may be sent and summed in bfloat16 or wider, within the bound.
A program may use at most 64 MiB of HBM per device.

v0:
```python
import functools

import jax
import jax.numpy as jnp
from jax import lax
from jax.experimental import pallas as pl
from jax.experimental.pallas import tpu as pltpu
from jax.sharding import PartitionSpec as P

P_SIZE = 64
N = 128
TAPS = 4
DRAFT_TOKENS = 5
MESH = pl.DeviceIdType.MESH
HIGH = lax.Precision.HIGHEST
f32, bf16 = jnp.float32, jnp.bfloat16
epsilon = 1e-05
VMEM_BYTES = 67043328


def factor(count):
    low = max(d for d in range(1, count + 1) if count % d == 0 and d * d <= count)
    return count // low, low


def remote(src, dst, send, recv, where):
    return pltpu.make_async_remote_copy(
        src_ref=src, dst_ref=dst, send_sem=send, recv_sem=recv, device_id=where, device_id_type=MESH
    )


def greet(places):
    barrier = pltpu.get_barrier_semaphore()
    for place in places:
        pl.semaphore_signal(barrier, inc=1, device_id=place, device_id_type=MESH)
    pl.semaphore_wait(barrier, len(places))


def project_kernel(
    nz, ny, own, model_width,
    tokens_h, gain_h, in_h, gate_h, write_h, read_h, step_h, bias_h, decay_h, extra_h,
    fresh_in, fresh_gate, fresh_write, fresh_read, steps_out, logs_out,
    tokens, gain, w_in, w_gate, w_write, w_read, step_block, bias, decay, extra,
    wide, ordered, tot, load_sem, *rest,
):
    pieces = 5
    send_y, recv_y, send_a, send_b, recv_a, recv_b = [
        rest[i * pieces : (i + 1) * pieces] for i in range(6)
    ]
    sy, ry, sza, rza, szb, rzb = rest[6 * pieces :]
    me = lax.axis_index("kv")
    col = lax.axis_index("tp")
    z, y = me // ny, lax.rem(me, ny)
    width = tokens.shape[1]
    heads = bias.shape[1]
    head_rows = own - own % 16
    half = w_in.shape[1] // 2
    step_cut = step_h.at[:, pl.ds(pl.multiple_of(me * width, 128), width)]
    loads = [
        pltpu.make_async_copy(source, target, load_sem.at[i])
        for i, (source, target) in enumerate((
            (tokens_h, tokens), (gain_h, gain), (step_cut, step_block), (write_h, w_write),
            (read_h, w_read), (in_h, w_in), (gate_h, w_gate), (bias_h, bias),
            (decay_h, decay), (extra_h, extra),
        ))
    ]
    for load in loads:
        load.start()
    y_peers = [z * ny + lax.rem(y + d, ny) for d in range(1, ny)]
    z_peers = [lax.rem(z + d, nz) * ny + y for d in range(1, nz)]
    barrier = pltpu.get_barrier_semaphore()
    for peer in y_peers + z_peers:
        pl.semaphore_signal(barrier, inc=1, device_id={"kv": peer}, device_id_type=MESH)

    loads[0].wait()
    loads[1].wait()
    wide[...] = tokens[...].astype(f32)
    for yy in range(ny):
        for zz in range(nz):
            at = (yy * nz + zz) * own
            source = (zz * ny + yy) * own
            ordered[at : at + own] = wide[source : source + own]
    values = ordered[...]
    squares = jnp.sum(values * values, axis=1, keepdims=True)
    scaled = (values * gain[...]).astype(bf16)
    block = nz * own
    for load in loads[2:5]:
        load.wait()
    picked_row = lax.broadcasted_iota(jnp.int32, (128, step_block.shape[0]), 0)
    pick = (
        lax.broadcasted_iota(jnp.int32, (128, step_block.shape[0]), 1) == picked_row + col * heads
    ) & (picked_row < heads)
    picked = jnp.dot(
        pick.astype(f32).astype(bf16), step_block[...], preferred_element_type=f32
    ).astype(bf16)
    lane = lax.broadcasted_iota(jnp.int32, (block, 128), 1)
    sw = w_write.shape[1]

    def start_y(piece):
        copies = []
        for d in range(1, ny):
            copy = remote(
                send_y[piece].at[lax.rem(y + d, ny)], recv_y[piece].at[d - 1],
                sy.at[piece, d - 1], ry.at[piece, d - 1], {"kv": y_peers[d - 1]},
            )
            copy.start()
            copies.append(copy)
        return copies

    y_copies = []
    for piece in range(pieces):
        if piece == 1:
            loads[5].wait()
        if piece == 3:
            loads[6].wait()
        for yy in range(ny):
            rows = scaled[yy * block : (yy + 1) * block]
            if piece == 0:
                send_y[0][yy, :, :sw] = jnp.dot(rows, w_write[...], preferred_element_type=f32).astype(bf16)
                send_y[0][yy, :, sw : 2 * sw] = jnp.dot(rows, w_read[...], preferred_element_type=f32).astype(bf16)
                term = lax.dot_general(
                    rows, picked, (((1,), (1,)), ((), ())), preferred_element_type=f32
                )
                term = jnp.where(lane == heads, squares[yy * block : (yy + 1) * block], term)
                send_y[0][yy, :, 2 * sw :] = term.astype(bf16)
            else:
                weight = w_in if piece < 3 else w_gate
                first = (piece - 1) % 2 * half
                send_y[piece][yy] = jnp.dot(
                    rows, weight[:, first : first + half], preferred_element_type=f32
                ).astype(bf16)
        if piece == 0:
            pl.semaphore_wait(barrier, len(y_peers) + len(z_peers))
        y_copies.append(start_y(piece))

    z_copies = []
    for piece in range(pieces):
        for copy in y_copies[piece]:
            copy.wait_recv()
        total = send_y[piece][y].astype(f32)
        for d in range(1, ny):
            total = total + recv_y[piece][d - 1].astype(f32)
        cw = total.shape[1]
        tot[:, :cw] = total
        for zz in range(nz):
            at = zz * own
            send_a[piece][zz] = tot[at : at + head_rows, :cw].astype(bf16)
            send_b[piece][zz] = tot[at + head_rows : at + own, :cw].astype(bf16)
        copies = []
        for d in range(1, nz):
            to = lax.rem(z + d, nz)
            for buf, landing, ss, rs in (
                (send_a, recv_a, sza, rza), (send_b, recv_b, szb, rzb)
            ):
                copy = remote(
                    buf[piece].at[to], landing[piece].at[d - 1],
                    ss.at[piece, d - 1], rs.at[piece, d - 1], {"kv": z_peers[d - 1]},
                )
                copy.start()
                copies.append(copy)
        z_copies.append(copies)

    for load in loads[7:]:
        load.wait()
    inverse = None
    seqs = own // DRAFT_TOKENS
    lead = TAPS - 1
    for piece in range(pieces):
        for copy in z_copies[piece]:
            copy.wait_recv()
        total_a = send_a[piece][z].astype(f32)
        total_b = send_b[piece][z].astype(f32)
        for d in range(1, nz):
            total_a = total_a + recv_a[piece][d - 1].astype(f32)
            total_b = total_b + recv_b[piece][d - 1].astype(f32)
        cw = total_a.shape[1]
        tot[:head_rows, :cw] = total_a
        tot[head_rows:own, :cw] = total_b
        full = tot[:own, :cw]
        if piece == 0:
            tailing = full[:, 2 * sw :]
            inverse = lax.rsqrt(tailing[:, heads : heads + 1] / model_width + epsilon)
            raw = tailing[:, :heads] * inverse
            steps = jax.nn.softplus(raw + bias[...])
            same_row = lax.broadcasted_iota(jnp.int32, (own, own), 0) == lax.broadcasted_iota(
                jnp.int32, (own, own), 1
            )
            added_logs = lax.dot_general(
                same_row.astype(f32), extra[...], (((1,), (1,)), ((), ())),
                precision=HIGH, preferred_element_type=f32,
            )
            logs = -steps * jnp.exp(decay[...]) + added_logs
            fresh = (full[:, : 2 * sw] * inverse).astype(bf16).astype(f32)
            steps_out[...] = jnp.zeros_like(steps_out)
            logs_out[...] = jnp.zeros_like(logs_out)
            fresh_write[...] = jnp.zeros_like(fresh_write)
            fresh_read[...] = jnp.zeros_like(fresh_read)
            for s in range(seqs):
                cut = slice(s * DRAFT_TOKENS, (s + 1) * DRAFT_TOKENS)
                steps_out[s, :DRAFT_TOKENS] = steps[cut]
                logs_out[s, :DRAFT_TOKENS] = logs[cut]
                fresh_write[s, lead : lead + DRAFT_TOKENS] = fresh[cut, :sw]
                fresh_read[s, lead : lead + DRAFT_TOKENS] = fresh[cut, sw:]
        else:
            fresh = (full * inverse).astype(bf16).astype(f32)
            target = fresh_in if piece < 3 else fresh_gate
            first = lead if piece < 3 else 0
            if piece % 2 == 1:
                target[...] = jnp.zeros_like(target)
            columns = slice((piece - 1) % 2 * half, (piece - 1) % 2 * half + half)
            for s in range(seqs):
                cut = slice(s * DRAFT_TOKENS, (s + 1) * DRAFT_TOKENS)
                target[s, first : first + DRAFT_TOKENS, columns] = fresh[cut]
    for copies in y_copies + z_copies:
        for copy in copies:
            copy.wait_send()


def state_kernel(
    group_width,
    accepted,
    fresh_in, fresh_gate, fresh_write, fresh_read, steps, logs,
    in_kernel, write_kernel, read_kernel, bypass, gain,
    saved_in, saved_write, saved_read, history,
    states, next_in, next_write, next_read, normed,
):
    taken = accepted[pl.program_id(0)]
    rows = DRAFT_TOKENS + TAPS - 1
    heads = steps.shape[2]
    width = in_kernel.shape[1]
    picks = (
        (lax.broadcasted_iota(jnp.int32, (rows, rows), 1)
         == lax.broadcasted_iota(jnp.int32, (rows, rows), 0) + taken)
        & (lax.broadcasted_iota(jnp.int32, (rows, rows), 0) < TAPS - 1)
    ).astype(f32).astype(bf16)

    def convolve(saved, fresh, taps, out):
        window = jnp.dot(picks, saved[0], preferred_element_type=f32) + fresh[0]
        out[0] = window.astype(bf16)
        total = taps[0:1] * window
        for k in range(1, TAPS):
            total = total + taps[k : k + 1] * pltpu.roll(window, rows - k, 0)
        return jax.nn.silu(total)

    x = convolve(saved_in, fresh_in, in_kernel, next_in)
    w = convolve(saved_write, fresh_write, write_kernel, next_write)
    r = convolve(saved_read, fresh_read, read_kernel, next_read)
    row = lax.broadcasted_iota(jnp.int32, (rows, heads), 0)
    log = logs[0]
    decay = jnp.zeros_like(log)
    for t in range(DRAFT_TOKENS):
        decay = decay + jnp.where(row >= t, log[t : t + 1], 0.0)
    keep = jnp.exp(decay)
    spread = (
        lax.broadcasted_iota(jnp.int32, (heads, width), 0)
        == lax.broadcasted_iota(jnp.int32, (heads, width), 1) // P_SIZE
    ).astype(f32)
    expand = functools.partial(jnp.dot, precision=HIGH, preferred_element_type=f32)
    decay_e = expand(decay, spread)
    step_x = expand(steps[0], spread) * x
    wide_row = lax.broadcasted_iota(jnp.int32, (rows, width), 0)
    direct = expand(jnp.broadcast_to(bypass[...], (rows, heads)), spread) * x
    groups = width // group_width
    per_group = group_width // P_SIZE
    gate = fresh_gate[0]
    gate = gate * jax.nn.sigmoid(gate)
    for g in range(groups):
        cut = slice(g * group_width, (g + 1) * group_width)
        wg, rg = w[:, g * N : (g + 1) * N], r[:, g * N : (g + 1) * N]
        hs = slice(g * per_group, (g + 1) * per_group)
        start = history[0, 0, hs].reshape(group_width, N)
        y = lax.dot_general(
            rg.astype(bf16), start.astype(bf16), (((1,), (1,)), ((), ())),
            preferred_element_type=f32,
        )
        dg, sg, mask_row = decay_e[:, cut], step_x[:, cut], wide_row[:, cut]
        y = y * jnp.exp(dg) + direct[:, cut]
        overlap = lax.dot_general(
            rg, wg, (((1,), (1,)), ((), ())), precision=HIGH, preferred_element_type=f32
        )
        for j in range(DRAFT_TOKENS):
            live = mask_row >= j
            fade = jnp.exp(jnp.where(live, dg - dg[j : j + 1], 0.0))
            y = y + jnp.where(live, fade * overlap[:, j : j + 1] * sg[j : j + 1], 0.0)
        gated = y * gate[:, cut]
        gated = gated * lax.rsqrt(jnp.mean(gated * gated, axis=1, keepdims=True) + epsilon)
        normed[0, :, cut] = gated * gain[:, cut]
        terms = []
        sides = []
        wide_w = jnp.concatenate([wg] * DRAFT_TOKENS, axis=1)
        lane = lax.broadcasted_iota(jnp.int32, wide_w.shape, 1) // N
        for t in range(DRAFT_TOKENS):
            live = mask_row <= t
            fade = jnp.exp(jnp.where(live, dg[t : t + 1] - dg, 0.0))
            terms.append(jnp.where(live, fade * sg, 0.0))
            sides.append(jnp.where(lane == t, wide_w, 0.0))
        left = jnp.concatenate(terms, axis=0).T.astype(bf16)
        added = jnp.dot(
            left, jnp.concatenate(sides, axis=0).astype(bf16), preferred_element_type=f32
        )
        for i in range(per_group):
            h = g * per_group + i
            own = history[0, 0, h]
            states[0, 0, h] = own
            for t in range(DRAFT_TOKENS):
                factor_th = jnp.broadcast_to(keep[t : t + 1, h : h + 1], (P_SIZE, N))
                states[0, t + 1, h] = (
                    factor_th * own
                    + added[i * P_SIZE : (i + 1) * P_SIZE, t * N : (t + 1) * N]
                )


def output_kernel(
    nz, ny, nt, own,
    normed, matrix, out,
    weight, rows_own, all_a, all_b, rows_b, send_a, send_b, recv_a, recv_b, final,
    w_sem, sz, rz, sy, ry, st, rt,
):
    me = lax.axis_index("kv")
    col = lax.axis_index("tp")
    z, y = me // ny, lax.rem(me, ny)
    w_copy = pltpu.make_async_copy(matrix, weight, w_sem)
    w_copy.start()
    head_rows = own - own % 16
    tail_rows = own - head_rows
    y_peers = [{"kv": z * ny + lax.rem(y + d, ny)} for d in range(1, ny)]
    z_peers = [{"kv": lax.rem(z + d, nz) * ny + y} for d in range(1, nz)]
    t_peers = [{"tp": lax.rem(col + d, nt)} for d in range(1, nt)]
    for s in range(own // DRAFT_TOKENS):
        rows_own[s * DRAFT_TOKENS : (s + 1) * DRAFT_TOKENS] = normed[s, :DRAFT_TOKENS]
    all_a[me] = rows_own[:head_rows].astype(bf16)
    all_b[me] = rows_own[head_rows:own].astype(bf16)
    greet(y_peers + z_peers + t_peers)

    def push(chunk, sends, recvs, place):
        pair = [
            remote(buf.at[chunk], buf.at[chunk], sends.at[i], recvs.at[i], place)
            for i, buf in enumerate((all_a, all_b))
        ]
        for copy in pair:
            copy.start()
        return pair

    z_copies = [push(me, sz.at[d], rz.at[d], z_peers[d]) for d in range(nz - 1)]
    y_sent = [push(me, sy.at[0, d], ry.at[0, d], y_peers[d]) for d in range(ny - 1)]
    for d in range(1, nz):
        for copy in z_copies[d - 1]:
            copy.wait_recv()
        chunk = lax.rem(z - d + nz, nz) * ny + y
        y_sent += [push(chunk, sy.at[d, e], ry.at[d, e], y_peers[e]) for e in range(ny - 1)]
    w_copy.wait()
    for pair in y_sent:
        for copy in pair:
            copy.wait_recv()
    for k in range(nz * ny):
        rows_b[k * tail_rows : (k + 1) * tail_rows] = all_b[k].astype(f32)
    left_a = all_a[...].reshape(nz * ny * head_rows, all_a.shape[2])
    part_a = jnp.dot(left_a, weight[...], preferred_element_type=f32)
    part_b = jnp.dot(rows_b[...].astype(bf16), weight[...], preferred_element_type=f32)
    each = nz * ny // nt
    for t in range(nt):
        send_a[t] = part_a[t * each * head_rows : (t + 1) * each * head_rows].astype(bf16)
        send_b[t] = part_b[t * each * tail_rows : (t + 1) * each * tail_rows].astype(bf16)
    t_copies = []
    for d in range(1, nt):
        to = lax.rem(col + d, nt)
        for i, (buf, landing) in enumerate(((send_a, recv_a), (send_b, recv_b))):
            copy = remote(
                buf.at[to], landing.at[d - 1], st.at[d - 1, i], rt.at[d - 1, i], t_peers[d - 1]
            )
            copy.start()
            t_copies.append(copy)
    total_a = send_a[col].astype(f32)
    total_b = send_b[col].astype(f32)
    for copy in t_copies:
        copy.wait_recv()
    for d in range(1, nt):
        total_a = total_a + recv_a[d - 1].astype(f32)
        total_b = total_b + recv_b[d - 1].astype(f32)
    for k in range(each):
        final[k * own : k * own + head_rows] = total_a[k * head_rows : (k + 1) * head_rows]
        final[k * own + head_rows : (k + 1) * own] = total_b[k * tail_rows : (k + 1) * tail_rows]
    out[...] = final[...].astype(bf16)
    for pair in z_copies + y_sent:
        for copy in pair:
            copy.wait_send()
    for copy in t_copies:
        copy.wait_send()


def per_device(
    tokens, input_norm_gain, input_matrix, gate_matrix, write_matrix, read_matrix, step_matrix,
    input_kernel, write_kernel, read_kernel, step_size_bias, head_decay_logs, bypass_scale,
    extra_decay_logs, output_norm_gain, output_matrix, cached_state_history,
    cached_input_rows, cached_write_rows, cached_read_rows, accepted,
):
    kv = lax.axis_size("kv")
    nt = lax.axis_size("tp")
    nz, ny = factor(kv)
    own = tokens.shape[0] // kv
    head_rows = own - own % 16
    tail_rows = own - head_rows
    seqs = own // DRAFT_TOKENS
    rows = DRAFT_TOKENS + TAPS - 1
    local = tokens.shape[1]
    heads = step_size_bias.shape[0]
    width = input_matrix.shape[1]
    sw = write_matrix.shape[1]
    vmem = pl.BlockSpec(memory_space=pltpu.VMEM)
    hbm = pl.BlockSpec(memory_space=pl.ANY)
    sizes = (2 * sw + 128,) + (width // 2,) * 4
    dma = pltpu.SemaphoreType.DMA
    peers = max(ny - 1, 1)
    shape = jax.ShapeDtypeStruct
    fresh_in, fresh_gate, fresh_write, fresh_read, steps, logs = pl.pallas_call(
        functools.partial(project_kernel, nz, ny, own, local * kv),
        out_shape=(
            shape((seqs, rows, width), f32), shape((seqs, rows, width), f32),
            shape((seqs, rows, sw), f32), shape((seqs, rows, sw), f32),
            shape((seqs, rows, heads), f32), shape((seqs, rows, heads), f32),
        ),
        in_specs=[hbm] * 10,
        out_specs=[vmem] * 6,
        scratch_shapes=[
            pltpu.VMEM(tokens.shape, bf16),
            pltpu.VMEM((1, local), f32),
            pltpu.VMEM((local, width), bf16),
            pltpu.VMEM((local, width), bf16),
            pltpu.VMEM((local, sw), bf16),
            pltpu.VMEM((local, sw), bf16),
            pltpu.VMEM((step_matrix.shape[1], local), bf16),
            pltpu.VMEM((1, heads), f32),
            pltpu.VMEM((1, heads), f32),
            pltpu.VMEM((heads, own), f32),
            pltpu.VMEM((tokens.shape[0], local), f32),
            pltpu.VMEM((tokens.shape[0], local), f32),
            pltpu.VMEM((nz * own, max(sizes)), f32),
            dma((10,)),
        ]
        + [pltpu.VMEM((ny, nz * own, c), bf16) for c in sizes]
        + [pltpu.VMEM((peers, nz * own, c), bf16) for c in sizes]
        + [pltpu.VMEM((nz, head_rows, c), bf16) for c in sizes]
        + [pltpu.VMEM((nz, tail_rows, c), bf16) for c in sizes]
        + [pltpu.VMEM((nz - 1, head_rows, c), bf16) for c in sizes]
        + [pltpu.VMEM((nz - 1, tail_rows, c), bf16) for c in sizes]
        + [dma((5, peers))] * 2
        + [dma((5, nz - 1))] * 4,
        compiler_params=pltpu.CompilerParams(
            collective_id=0, has_side_effects=True, vmem_limit_bytes=VMEM_BYTES
        ),
    )(
        tokens, input_norm_gain[None], input_matrix, gate_matrix, write_matrix, read_matrix,
        step_matrix.T, step_size_bias[None], head_decay_logs[None], extra_decay_logs.T,
    )

    def per_seq(*dims):
        return pl.BlockSpec((1,) + dims, lambda s, acc: (s,) + (0,) * len(dims))

    def same(*dims):
        return pl.BlockSpec(dims, lambda s, acc: (0,) * len(dims))

    group_width = width // (sw // N)
    next_states, next_input, next_write, next_read, normed = pl.pallas_call(
        functools.partial(state_kernel, group_width),
        grid_spec=pltpu.PrefetchScalarGridSpec(
            num_scalar_prefetch=1,
            grid=(seqs,),
            in_specs=[
                per_seq(rows, width), per_seq(rows, width), per_seq(rows, sw), per_seq(rows, sw),
                per_seq(rows, heads), per_seq(rows, heads),
                same(TAPS, width), same(TAPS, sw), same(TAPS, sw), same(1, heads), same(1, width),
                per_seq(rows, width), per_seq(rows, sw), per_seq(rows, sw),
                pl.BlockSpec((1, 1, heads, P_SIZE, N), lambda s, acc: (s, acc[s], 0, 0, 0)),
            ],
            out_specs=[
                per_seq(DRAFT_TOKENS + 1, heads, P_SIZE, N),
                per_seq(rows, width), per_seq(rows, sw), per_seq(rows, sw), per_seq(rows, width),
            ],
        ),
        out_shape=(
            shape(cached_state_history.shape, f32),
            shape(cached_input_rows.shape, bf16),
            shape(cached_write_rows.shape, bf16),
            shape(cached_read_rows.shape, bf16),
            shape((seqs, rows, width), f32),
        ),
        compiler_params=pltpu.CompilerParams(vmem_limit_bytes=VMEM_BYTES),
    )(
        accepted, fresh_in, fresh_gate, fresh_write, fresh_read, steps, logs,
        input_kernel, write_kernel, read_kernel, bypass_scale[None], output_norm_gain[None],
        cached_input_rows, cached_write_rows, cached_read_rows, cached_state_history,
    )

    out_width = output_matrix.shape[1]
    each = kv // nt
    mixer_out = pl.pallas_call(
        functools.partial(output_kernel, nz, ny, nt, own),
        out_shape=shape((each * own, out_width), bf16),
        in_specs=[vmem, hbm],
        out_specs=vmem,
        scratch_shapes=[
            pltpu.VMEM(output_matrix.shape, bf16),
            pltpu.VMEM((own, width), f32),
            pltpu.VMEM((kv, head_rows, width), bf16),
            pltpu.VMEM((kv, tail_rows, width), bf16),
            pltpu.VMEM((kv * tail_rows, width), f32),
            pltpu.VMEM((nt, each * head_rows, out_width), bf16),
            pltpu.VMEM((nt, each * tail_rows, out_width), bf16),
            pltpu.VMEM((nt - 1, each * head_rows, out_width), bf16),
            pltpu.VMEM((nt - 1, each * tail_rows, out_width), bf16),
            pltpu.VMEM((each * own, out_width), f32),
            dma(()),
            dma((nz - 1, 2)), dma((nz - 1, 2)),
            dma((nz, peers, 2)), dma((nz, peers, 2)),
            dma((nt - 1, 2)), dma((nt - 1, 2)),
        ],
        compiler_params=pltpu.CompilerParams(
            collective_id=1, has_side_effects=True, vmem_limit_bytes=VMEM_BYTES
        ),
    )(normed, output_matrix)
    return mixer_out, next_states, next_input, next_write, next_read


def solution(mesh):
    return jax.shard_map(
        per_device,
        mesh=mesh,
        in_specs=(
            P(None, "kv"),
            P("kv"),
            P("kv", "tp"),
            P("kv", "tp"),
            P("kv", "tp"),
            P("kv", "tp"),
            P(),
            P(None, "tp"),
            P(None, "tp"),
            P(None, "tp"),
            P("tp"),
            P("tp"),
            P("tp"),
            P("kv", "tp"),
            P("tp"),
            P("tp", "kv"),
            P("kv", None, "tp", None, None),
            P("kv", None, "tp"),
            P("kv", None, "tp"),
            P("kv", None, "tp"),
            P("kv"),
        ),
        out_specs=(
            P("tp", "kv"),
            P("kv", None, "tp", None, None),
            P("kv", None, "tp"),
            P("kv", None, "tp"),
            P("kv", None, "tp"),
        ),
        check_vma=False,
    )
```

profile of v0, /device:TPU:0, one launch (start us, length us, event | category | flops | bytes accessed | tf_op | source)
XLA Modules:
  0.0 48.0 jit_solution(2044862843303439113)
XLA Ops:
  0.6 21.4 %shard_map.236 = (f32[4,8,1024]{2,1,0:T(8,128)}, f32[4,8,1024]{2,1,0:T(8,128)}, f32[4,8,256]{2,1,0:T(8,128)}, f32[4,8,256]{2,1,0:T(8,128)}, f32[4,8,16]{2,1,0:T(8,128)}, /*index=5*/f32[4,8,16]{2,1,0:T(8,128)}) custom-call(bf16[160,512]{1,0:T(8,128)(2,1)} %tokens_h.1, f32[1,512]{1,0:T(1,128)} %bitcast.10, bf16[512,1024]{1,0:T(8,128)(2,1)} %in_h.1, ...), custom_call_target="tpu_custom_call" | custom-call | tf_op jit(solution)/shard_map/pallas_call | solution.py:415
  22.1 9.0 %shard_map.237 = (f32[4,6,16,64,128]{4,3,2,1,0:T(8,128)}, bf16[4,8,1024]{2,1,0:T(8,128)(2,1)}, bf16[4,8,256]{2,1,0:T(8,128)(2,1)}, bf16[4,8,256]{2,1,0:T(8,128)(2,1)}, f32[4,8,1024]{2,1,0:T(8,128)}) custom-call(s32[4]{0:T(128)} %accepted.1, f32[4,8,1024]{2,1,0:T(8,128)} %get-tuple-element.16.fresh_in, f32[4,8,1024]{2,1,0:T(8,128)} %get-tuple-element.17.fresh_gate, ...), custom_call_target="tpu_custom_call" | custom-call | tf_op jit(solution)/shard_map/pallas_call | solution.py:463
  31.1 15.5 %shard_map.238 = bf16[40,512]{1,0:T(8,128)(2,1)} custom-call(f32[4,8,1024]{2,1,0:T(8,128)} %get-tuple-element.22.normed, bf16[1024,512]{1,0:T(8,128)(2,1)} %matrix.1), custom_call_target="tpu_custom_call" | custom-call | tf_op jit(solution)/shard_map/pallas_call | solution.py:496
  46.6 1.4 %copy.27 = bf16[40,512]{1,0:T(8,128)(2,1)} copy(bf16[40,512]{1,0:T(8,128)(2,1)} %shard_map.238) | data formatting | bytes 81920
where the time goes:
time: 48.4 us; the launch traced here: 48 us
  Pallas kernels  46 us (95%)
  local copies, waits for them, and re-layouts  1.4 us (3%)
  between operations  0.66 us (1%)
    pallas_call x1, Pallas kernels, per_device(): pl.pallas_call(functools.partial(project_kernel, nz, ny, own, local * kv)...  21.4 us
    pallas_call x1, Pallas kernels, per_device(): pl.pallas_call(functools.partial(output_kernel, nz, ny, nt, own), out_sha...  15.5 us
    pallas_call x1, Pallas kernels, per_device(): pl.pallas_call(functools.partial(state_kernel, group_width), grid_spec=pl...  9.04 us
    unnamed x1, local copies, waits for them, and re-layouts  1.4 us

commit v1 on v0

v1 whole, which is shorter than its diff:
```python
import functools

import jax
import jax.numpy as jnp
from jax import lax
from jax.experimental import pallas as pl
from jax.experimental.pallas import tpu as pltpu
from jax.sharding import PartitionSpec as P

P_SIZE = 64
N = 128
TAPS = 4
DRAFT_TOKENS = 5
ROWS = DRAFT_TOKENS + TAPS - 1
LEAD = TAPS - 1
MESH = pl.DeviceIdType.MESH
HIGH = lax.Precision.HIGHEST
f32, bf16 = jnp.float32, jnp.bfloat16
epsilon = 1e-05


def factor(count):
    low = max(d for d in range(1, count + 1) if count % d == 0 and d * d <= count)
    return count // low, low


def paired(count):
    return count in (1, 2, 4)


def peer_to(me, d, count):
    if not paired(count):
        return lax.rem(me + d, count)
    if d == count // 2:
        return lax.rem(me + d, count)
    if d == count - 1:
        return count - 1 - me
    return me + 1 - 2 * lax.rem(me, 2)


def peer_from(me, d, count):
    if not paired(count):
        return lax.rem(me - d + count, count)
    return peer_to(me, d, count)


def remote(src, dst, send, recv, where):
    return pltpu.make_async_remote_copy(
        src_ref=src, dst_ref=dst, send_sem=send, recv_sem=recv, device_id=where, device_id_type=MESH
    )


def iota(shape, dim):
    return lax.broadcasted_iota(jnp.int32, shape, dim)


def one_hot(mask):
    return mask.astype(f32).astype(bf16)


def dot(a, b, **more):
    return jnp.dot(a, b, preferred_element_type=f32, **more)


def mixer_kernel(
    nz, ny, nt, own, model_width, plan, group_width,
    tokens_h, gain_h, in_h, gate_h, write_h, read_h, step_h, bias_h, decay_h, extra_h,
    in_taps_h, write_taps_h, read_taps_h, bypass_h, out_gain_h, matrix_h,
    history_h, saved_in_h, saved_write_h, saved_read_h, accepted_h,
    mix, states, next_in, next_write, next_read,
    tokens, gain, w_in, w_gate, w_write, w_read, step_block, bias, decay, extra,
    in_taps, write_taps, read_taps, bypass, out_gain, matrix,
    history, saved_in, saved_write, saved_read, accepted, load_sem,
    wide, ordered, scaled, tail_squares, own_part, tot, tot_own, y_all, keep_all, decay_all,
    step_all, w_all,
    all_a, all_b, rows_b, out_a, out_b, land_a, land_b, final,
    sy, ry, sz, rz, gz_s, gz_r, gy_s, gy_r, st, rt, *rest,
):
    pieces = len(plan)
    send_y, recv_y, send_a, send_b, recv_a, recv_b = [
        rest[i * pieces : (i + 1) * pieces] for i in range(6)
    ]
    me = lax.axis_index("kv")
    col = lax.axis_index("tp")
    z, y = me // ny, lax.rem(me, ny)
    width = w_in.shape[1]
    sw = w_write.shape[1]
    local = tokens.shape[1]
    heads = bias.shape[1]
    seqs = own // DRAFT_TOKENS
    head_rows = own - own % 16
    tail_rows = own - head_rows
    block = nz * own
    full_rows = seqs * ROWS
    pad = tot_own.shape[0]
    groups = width // group_width
    per_group = group_width // P_SIZE

    step_cut = step_h.at[:, pl.ds(pl.multiple_of(me * local, 128), local)]
    pairs = [
        (tokens_h, tokens), (gain_h, gain), (step_cut, step_block), (write_h, w_write),
        (read_h, w_read), (in_h, w_in), (gate_h, w_gate), (bias_h, bias),
        (decay_h, decay), (extra_h, extra), (accepted_h, accepted),
        (saved_in_h, saved_in), (saved_write_h, saved_write), (saved_read_h, saved_read),
        (in_taps_h, in_taps), (write_taps_h, write_taps), (read_taps_h, read_taps),
        (bypass_h, bypass), (out_gain_h, out_gain), (matrix_h, matrix),
    ] + [(history_h.at[s], history.at[s]) for s in range(seqs)]
    loads = [
        pltpu.make_async_copy(source, target, load_sem.at[i])
        for i, (source, target) in enumerate(pairs)
    ]
    for load in loads[:11]:
        load.start()
    y_to = [{"kv": z * ny + lax.rem(y + d, ny)} for d in range(1, ny)]
    z_to = [{"kv": peer_to(z, d, nz) * ny + y} for d in range(1, nz)]
    t_to = [{"tp": peer_to(col, d, nt)} for d in range(1, nt)]
    barrier = pltpu.get_barrier_semaphore()
    for peer in y_to + z_to + t_to:
        pl.semaphore_signal(barrier, inc=1, device_id=peer, device_id_type=MESH)
    for load in loads[11:]:
        load.start()

    loads[0].wait()
    loads[1].wait()
    wide[...] = tokens[...].astype(f32)
    for yy in range(ny):
        for zz in range(nz):
            source = (zz * ny + yy) * own
            at = zz * head_rows
            ordered[yy, at : at + head_rows] = wide[source : source + head_rows]
            if tail_rows:
                at = nz * head_rows + zz * tail_rows
                ordered[yy, at : at + tail_rows] = wide[source + head_rows : source + own]
    lane = iota((block, 128), 1)
    for yy in range(ny):
        values = ordered[yy]
        scaled[yy] = (values * gain[...]).astype(bf16)
        squares = jnp.sum(values * values, axis=1, keepdims=True)
        tail_squares[yy] = jnp.where(lane == heads, squares, 0.0)
    loads[2].wait()
    picked_row = iota((128, step_block.shape[0]), 0)
    pick = (iota((128, step_block.shape[0]), 1) == picked_row + col * heads) & (picked_row < heads)
    picked = dot(one_hot(pick), step_block[...]).astype(bf16)
    loads[3].wait()
    loads[4].wait()
    weights = {"in": w_in, "gate": w_gate}

    def project(kind, first, size, at):
        rows = scaled[at]
        if kind == "small":
            return [
                (0, dot(rows, w_write[...])), (sw, dot(rows, w_read[...])),
                (2 * sw, tail_squares[at] + lax.dot_general(
                    rows, picked, (((1,), (1,)), ((), ())), preferred_element_type=f32
                )),
            ]
        return [(0, dot(rows, weights[kind][:, first : first + size]))]

    y_copies = []
    for p, (kind, first, size) in enumerate(plan):
        if p > 0 and kind == "in" and first == 0:
            loads[5].wait()
        if kind == "gate" and first == 0:
            loads[6].wait()
        copies = []
        for d in range(1, ny):
            for at, part in project(kind, first, size, lax.rem(y + d, ny)):
                send_y[p][d - 1, :, at : at + part.shape[1]] = part.astype(bf16)
            if p == 0 and d == 1:
                pl.semaphore_wait(barrier, len(y_to) + len(z_to) + len(t_to))
            copy = remote(
                send_y[p].at[d - 1], recv_y[p].at[d - 1], sy.at[p, d - 1], ry.at[p, d - 1],
                y_to[d - 1],
            )
            copy.start()
            copies.append(copy)
        y_copies.append(copies)
    if ny == 1:
        pl.semaphore_wait(barrier, len(z_to) + len(t_to))

    offsets = []
    total_columns = 0
    for _, _, size in plan:
        offsets.append(total_columns)
        total_columns += size
    for p, (kind, first, size) in enumerate(plan):
        for at, part in project(kind, first, size, y):
            own_part[:, offsets[p] + at : offsets[p] + at + part.shape[1]] = part
    tot_own[...] = jnp.zeros_like(tot_own)

    z_copies = []
    for p, (_, _, size) in enumerate(plan):
        total = own_part[:, offsets[p] : offsets[p] + size]
        for d in range(1, ny):
            y_copies[p][d - 1].wait_recv()
            total = total + recv_y[p][d - 1].astype(f32)
        tot[:, :size] = total
        for zz in range(nz):
            at = zz * head_rows
            send_a[p][zz] = tot[at : at + head_rows, :size].astype(bf16)
            at = nz * head_rows + zz * tail_rows
            if tail_rows:
                send_b[p][zz] = tot[at : at + tail_rows, :size].astype(bf16)
        copies = []
        for d in reversed(range(1, nz)):
            to = peer_to(z, d, nz)
            for i, (buf, landing) in enumerate(((send_a, recv_a), (send_b, recv_b))):
                if i == 1 and not tail_rows:
                    continue
                copy = remote(
                    buf[p].at[to], landing[p].at[d - 1],
                    sz.at[p, d - 1, i], rz.at[p, d - 1, i], z_to[d - 1],
                )
                copy.start()
                copies.append(copy)
        z_copies.append(copies)

    row = iota((full_rows, pad), 0)
    column = iota((full_rows, pad), 1)
    seq_of, step_of = row // ROWS, lax.rem(row, ROWS)
    token = column - seq_of * DRAFT_TOKENS
    place_tok = one_hot((token == step_of) & (step_of < DRAFT_TOKENS))
    place_win = one_hot((token == step_of - LEAD) & (step_of >= LEAD))
    reach = ((token >= 0) & (token <= step_of) & (token < DRAFT_TOKENS)).astype(f32)
    square_row = iota((full_rows, full_rows), 0)
    square_column = iota((full_rows, full_rows), 1)
    for load in loads[7:19]:
        load.wait()
    taken = [accepted[s] for s in range(seqs)]
    shift = jnp.zeros((full_rows, full_rows), jnp.int32)
    for s in range(seqs):
        shift = jnp.where(square_row // ROWS == s, taken[s], shift)
    picks = one_hot(
        (square_column == square_row + shift) & (lax.rem(square_row, ROWS) < LEAD)
    )

    def gathered(p):
        size = plan[p][2]
        for copy in z_copies[p]:
            copy.wait_recv()
        total_a = send_a[p][z].astype(f32)
        for d in range(1, nz):
            total_a = total_a + recv_a[p][d - 1].astype(f32)
        tot_own[:head_rows, :size] = total_a
        if tail_rows:
            total_b = send_b[p][z].astype(f32)
            for d in range(1, nz):
                total_b = total_b + recv_b[p][d - 1].astype(f32)
            tot_own[head_rows:own, :size] = total_b
        return tot_own[:, :size]

    def convolve(saved, fresh, taps, out):
        kept = saved.astype(f32).reshape(full_rows, saved.shape[2]).astype(bf16)
        window = dot(picks, kept) + dot(place_win, fresh)
        window = window.reshape(seqs, ROWS, saved.shape[2])
        out(window.astype(bf16))
        total = taps[0:1][None] * window
        for k in range(1, TAPS):
            total = total + taps[k : k + 1][None] * pltpu.roll(window, ROWS - k, 1)
        return jax.nn.silu(total).reshape(full_rows, saved.shape[2])

    def store(ref, cut):
        def put(value):
            ref[:, :, cut] = value
        return put

    small = gathered(0)
    tailing = small[:, 2 * sw :]
    inverse = lax.rsqrt(tailing[:, heads : heads + 1] / model_width + epsilon)
    steps = jax.nn.softplus(tailing[:, :heads] * inverse + bias[...])
    fresh = (small[:, : 2 * sw] * inverse).astype(bf16)
    w = convolve(saved_write[...], fresh[:, :sw], write_taps[...], store(next_write, slice(0, sw)))
    r = convolve(saved_read[...], fresh[:, sw:], read_taps[...], store(next_read, slice(0, sw)))
    w_all[...] = w
    added_logs = lax.dot_general(
        (iota((pad, own), 0) == iota((pad, own), 1)).astype(f32), extra[...],
        (((1,), (1,)), ((), ())), precision=HIGH, preferred_element_type=f32,
    )
    logs = jnp.where(iota((pad, heads), 0) < own, -steps * jnp.exp(decay[...]) + added_logs, 0.0)
    summed = dot(reach, logs, precision=HIGH)
    steps_placed = dot(place_tok.astype(f32), steps, precision=HIGH)
    keep_all[...] = jnp.exp(summed)
    spread = (iota((heads, width), 0) == iota((heads, width), 1) // P_SIZE).astype(f32)
    stacked = jnp.concatenate(
        [summed, steps_placed, jnp.broadcast_to(bypass[...], (8, heads))], axis=0
    )
    spreaded = dot(stacked, spread, precision=HIGH)
    decay_all[...] = spreaded[:full_rows]
    step_all[...] = spreaded[full_rows : 2 * full_rows]
    direct = spreaded[2 * full_rows : 2 * full_rows + 1]
    mask_row = iota((ROWS, group_width), 0)
    for load in loads[20:]:
        load.wait()
    p_in = [p for p in range(pieces) if plan[p][0] == "in"]
    p_gate = [p for p in range(pieces) if plan[p][0] == "gate"]
    for g, p in enumerate(p_in):
        cut = slice(g * group_width, (g + 1) * group_width)
        fresh = (gathered(p) * inverse).astype(bf16)
        x = convolve(saved_in[:, :, cut], fresh, in_taps[:, cut], store(next_in, cut))
        step_x = step_all[:, cut] * x
        step_all[:, cut] = step_x
        through = direct[:, cut] * x
        for s in range(seqs):
            rs = slice(s * ROWS, (s + 1) * ROWS)
            wg, rg = w[rs, g * N : (g + 1) * N], r[rs, g * N : (g + 1) * N]
            start = history[s, taken[s], g * per_group : (g + 1) * per_group].reshape(group_width, N)
            out = lax.dot_general(
                rg.astype(bf16), start.astype(bf16), (((1,), (1,)), ((), ())),
                preferred_element_type=f32,
            )
            dg, sg = decay_all[rs, cut], step_x[rs]
            out = out * jnp.exp(dg) + through[rs]
            overlap = lax.dot_general(
                rg, wg, (((1,), (1,)), ((), ())), precision=HIGH, preferred_element_type=f32
            )
            for j in range(DRAFT_TOKENS):
                live = mask_row >= j
                fade = jnp.exp(jnp.where(live, dg - dg[j : j + 1], 0.0))
                out = out + jnp.where(live, fade * overlap[:, j : j + 1] * sg[j : j + 1], 0.0)
            y_all[rs, cut] = out

    def push(g, chunk, sends, recvs, place):
        pair = []
        for i, buf in enumerate((all_a, all_b)):
            if i == 0 or tail_rows:
                pair.append(remote(
                    buf.at[g, chunk], buf.at[g, chunk], sends.at[i], recvs.at[i], place
                ))
                pair[-1].start()
        return pair

    compact_row, compact_column = iota((pad, full_rows), 0), iota((pad, full_rows), 1)
    compact_step = lax.rem(compact_column, ROWS)
    compact = one_hot(
        (compact_row == compact_column // ROWS * DRAFT_TOKENS + compact_step)
        & (compact_step < DRAFT_TOKENS)
    )
    gz_copies, gy_copies = [], []
    for g in range(groups):
        cut = slice(g * group_width, (g + 1) * group_width)
        parts = []
        for p in p_gate:
            if cut.start <= plan[p][1] < cut.stop:
                parts.append(dot(place_tok, (gathered(p) * inverse).astype(bf16)))
        gate = parts[0] if len(parts) == 1 else jnp.concatenate(parts, axis=1)
        gated = y_all[:, cut] * (gate * jax.nn.sigmoid(gate))
        gated = gated * lax.rsqrt(jnp.mean(gated * gated, axis=1, keepdims=True) + epsilon)
        normed = dot(compact, (gated * out_gain[:, cut]).astype(bf16)).astype(bf16)
        all_a[g, me] = normed[:head_rows]
        if tail_rows:
            all_b[g, me] = normed[head_rows:own]
        gz_copies.append([
            push(g, me, gz_s.at[g, d - 1], gz_r.at[g, d - 1], z_to[d - 1])
            for d in reversed(range(1, nz))
        ][::-1])
        gy_copies.append([
            push(g, me, gy_s.at[g, 0, d], gy_r.at[g, 0, d], y_to[d]) for d in range(ny - 1)
        ])

    for s in range(seqs):
        rs = slice(s * ROWS, (s + 1) * ROWS)
        keep = keep_all[rs]
        for g in range(groups):
            cut = slice(g * group_width, (g + 1) * group_width)
            wg, dg, sg = w_all[rs, g * N : (g + 1) * N], decay_all[rs, cut], step_all[rs, cut]
            terms = []
            sides = []
            wide_w = jnp.concatenate([wg] * DRAFT_TOKENS, axis=1)
            wide_lane = iota(wide_w.shape, 1) // N
            for t in range(DRAFT_TOKENS):
                live = mask_row <= t
                fade = jnp.exp(jnp.where(live, dg[t : t + 1] - dg, 0.0))
                terms.append(jnp.where(live, fade * sg, 0.0))
                sides.append(jnp.where(wide_lane == t, wide_w, 0.0))
            left = jnp.concatenate(terms, axis=0).T.astype(bf16)
            added = dot(left, jnp.concatenate(sides, axis=0).astype(bf16))
            for i in range(per_group):
                h = g * per_group + i
                held = history[s, taken[s], h]
                states[s, 0, h] = held
                for t in range(DRAFT_TOKENS):
                    factor_th = jnp.broadcast_to(keep[t : t + 1, h : h + 1], (P_SIZE, N))
                    states[s, t + 1, h] = (
                        factor_th * held
                        + added[i * P_SIZE : (i + 1) * P_SIZE, t * N : (t + 1) * N]
                    )

    for g in range(groups):
        for d in range(1, nz):
            for copy in gz_copies[g][d - 1]:
                copy.wait_recv()
            chunk = peer_from(z, d, nz) * ny + y
            gy_copies[g] += [
                push(g, chunk, gy_s.at[g, d, e], gy_r.at[g, d, e], y_to[e]) for e in range(ny - 1)
            ]
    loads[19].wait()
    part_a, part_b = 0.0, 0.0
    for g in range(groups):
        for pair in gy_copies[g]:
            for copy in pair:
                copy.wait_recv()
        weight = matrix[g * group_width : (g + 1) * group_width]
        part_a = part_a + dot(all_a[g].reshape(nz * ny * head_rows, group_width), weight)
        if tail_rows:
            for k in range(nz * ny):
                rows_b[k * tail_rows : (k + 1) * tail_rows] = all_b[g, k].astype(f32)
            part_b = part_b + dot(rows_b[...].astype(bf16), weight)
    each = nz * ny // nt
    for t in range(nt):
        out_a[t] = part_a[t * each * head_rows : (t + 1) * each * head_rows].astype(bf16)
        if tail_rows:
            out_b[t] = part_b[t * each * tail_rows : (t + 1) * each * tail_rows].astype(bf16)
    t_copies = []
    for d in reversed(range(1, nt)):
        to = peer_to(col, d, nt)
        for i, (buf, landing) in enumerate(((out_a, land_a), (out_b, land_b))):
            if i == 0 or tail_rows:
                copy = remote(
                    buf.at[to], landing.at[d - 1], st.at[d - 1, i], rt.at[d - 1, i], t_to[d - 1]
                )
                copy.start()
                t_copies.append(copy)
    for copy in t_copies:
        copy.wait_recv()
    total_a = out_a[col].astype(f32)
    for d in range(1, nt):
        total_a = total_a + land_a[d - 1].astype(f32)
    if tail_rows:
        total_b = out_b[col].astype(f32)
        for d in range(1, nt):
            total_b = total_b + land_b[d - 1].astype(f32)
    for k in range(each):
        final[k * own : k * own + head_rows] = total_a[k * head_rows : (k + 1) * head_rows]
        if tail_rows:
            final[k * own + head_rows : (k + 1) * own] = (
                total_b[k * tail_rows : (k + 1) * tail_rows]
            )
    mix[...] = final[...].astype(bf16)
    for copies in y_copies + z_copies:
        for copy in copies:
            copy.wait_send()
    for pairs_of in gz_copies + gy_copies:
        for pair in pairs_of:
            for copy in pair:
                copy.wait_send()
    for copy in t_copies:
        copy.wait_send()


def emit_kernel(
    mix, states, next_in, next_write, next_read,
    mix_h, states_h, next_in_h, next_write_h, next_read_h, sem,
):
    pairs = [
        (states.at[s, t], states_h.at[s, t])
        for s in range(states.shape[0]) for t in range(states.shape[1])
    ] + [
        (mix, mix_h), (next_in, next_in_h), (next_write, next_write_h), (next_read, next_read_h),
    ]
    copies = [
        pltpu.make_async_copy(source, target, sem.at[i])
        for i, (source, target) in enumerate(pairs)
    ]
    for copy in copies:
        copy.start()
    for copy in copies:
        copy.wait()


def per_device(
    tokens, input_norm_gain, input_matrix, gate_matrix, write_matrix, read_matrix, step_matrix,
    input_kernel, write_kernel, read_kernel, step_size_bias, head_decay_logs, bypass_scale,
    extra_decay_logs, output_norm_gain, output_matrix, cached_state_history,
    cached_input_rows, cached_write_rows, cached_read_rows, accepted,
):
    kv = lax.axis_size("kv")
    nt = lax.axis_size("tp")
    nz, ny = factor(kv)
    own = tokens.shape[0] // kv
    head_rows = own - own % 16
    tail_rows = max(own - head_rows, 1)
    seqs = own // DRAFT_TOKENS
    full_rows = seqs * ROWS
    pad = -(-own // 16) * 16
    block = nz * own
    local = tokens.shape[1]
    heads = step_size_bias.shape[0]
    width = input_matrix.shape[1]
    sw = write_matrix.shape[1]
    group_width = width // (sw // N)
    groups = width // group_width
    half = group_width // 2
    out_width = output_matrix.shape[1]
    each = kv // nt
    vmem = pl.BlockSpec(memory_space=pltpu.VMEM)
    hbm = pl.BlockSpec(memory_space=pltpu.HBM)
    plan = [("small", 0, 2 * sw + 128)]
    plan += [("in", g * group_width, group_width) for g in range(groups)]
    plan += [("gate", g * group_width, group_width) for g in range(groups - 1)]
    last = (groups - 1) * group_width
    plan += [("gate", last, half), ("gate", last + half, half)]
    sizes = [size for _, _, size in plan]
    pieces = len(plan)
    dma = pltpu.SemaphoreType.DMA
    peers = max(ny - 1, 1)
    shape = jax.ShapeDtypeStruct
    operands = (
        tokens, input_norm_gain[None], input_matrix, gate_matrix, write_matrix, read_matrix,
        step_matrix.T, step_size_bias[None], head_decay_logs[None], extra_decay_logs.T,
        input_kernel, write_kernel, read_kernel, bypass_scale[None], output_norm_gain[None],
        output_matrix, cached_state_history, cached_input_rows, cached_write_rows,
        cached_read_rows, accepted,
    )
    step_shape = (step_matrix.shape[1], local)
    buffers = [
        pltpu.VMEM(step_shape if i == 6 else a.shape, a.dtype)
        for i, a in enumerate(operands[:-1])
    ]
    results = (
        ((each * own, out_width), bf16), (cached_state_history.shape, f32),
        (cached_input_rows.shape, bf16), (cached_write_rows.shape, bf16),
        (cached_read_rows.shape, bf16),
    )
    outs = pl.pallas_call(
        functools.partial(
            mixer_kernel, nz, ny, nt, own, local * kv, tuple(plan), group_width
        ),
        out_shape=tuple(pltpu.VMEM(dims, kind) for dims, kind in results),
        in_specs=[hbm] * len(operands),
        out_specs=[vmem] * len(results),
        scratch_shapes=buffers + [
            pltpu.SMEM(accepted.shape, jnp.int32),
            dma((len(operands) - 1 + seqs,)),
            pltpu.VMEM(tokens.shape, f32),
            pltpu.VMEM((ny, block, local), f32),
            pltpu.VMEM((ny, block, local), bf16),
            pltpu.VMEM((ny, block, 128), f32),
            pltpu.VMEM((block, sum(sizes)), f32),
            pltpu.VMEM((block, max(sizes)), f32),
            pltpu.VMEM((pad, max(sizes)), f32),
            pltpu.VMEM((full_rows, width), f32),
            pltpu.VMEM((full_rows, heads), f32),
            pltpu.VMEM((full_rows, width), f32),
            pltpu.VMEM((full_rows, width), f32),
            pltpu.VMEM((full_rows, sw), f32),
            pltpu.VMEM((groups, kv, head_rows, group_width), bf16),
            pltpu.VMEM((groups, kv, tail_rows, group_width), bf16),
            pltpu.VMEM((kv * tail_rows, group_width), f32),
            pltpu.VMEM((nt, each * head_rows, out_width), bf16),
            pltpu.VMEM((nt, each * tail_rows, out_width), bf16),
            pltpu.VMEM((nt - 1, each * head_rows, out_width), bf16),
            pltpu.VMEM((nt - 1, each * tail_rows, out_width), bf16),
            pltpu.VMEM((each * own, out_width), f32),
            dma((pieces, peers)), dma((pieces, peers)),
            dma((pieces, nz - 1, 2)), dma((pieces, nz - 1, 2)),
            dma((groups, nz - 1, 2)), dma((groups, nz - 1, 2)),
            dma((groups, nz, peers, 2)), dma((groups, nz, peers, 2)),
            dma((nt - 1, 2)), dma((nt - 1, 2)),
        ]
        + [pltpu.VMEM((peers, block, c), bf16) for c in sizes]
        + [pltpu.VMEM((peers, block, c), bf16) for c in sizes]
        + [pltpu.VMEM((nz, head_rows, c), bf16) for c in sizes]
        + [pltpu.VMEM((nz, tail_rows, c), bf16) for c in sizes]
        + [pltpu.VMEM((nz - 1, head_rows, c), bf16) for c in sizes]
        + [pltpu.VMEM((nz - 1, tail_rows, c), bf16) for c in sizes],
        compiler_params=pltpu.CompilerParams(
            collective_id=0, has_side_effects=True, vmem_limit_bytes=40 * 2**20
        ),
    )(*[pltpu.with_memory_space_constraint(a, pltpu.HBM) for a in operands])
    return tuple(pl.pallas_call(
        emit_kernel,
        out_shape=tuple(shape(dims, kind) for dims, kind in results),
        in_specs=[vmem] * len(results),
        out_specs=[hbm] * len(results),
        scratch_shapes=[dma((seqs * (DRAFT_TOKENS + 1) + len(results) - 1,))],
        compiler_params=pltpu.CompilerParams(vmem_limit_bytes=2**20),
    )(*outs))


def solution(mesh):
    return jax.shard_map(
        per_device,
        mesh=mesh,
        in_specs=(
            P(None, "kv"),
            P("kv"),
            P("kv", "tp"),
            P("kv", "tp"),
            P("kv", "tp"),
            P("kv", "tp"),
            P(),
            P(None, "tp"),
            P(None, "tp"),
            P(None, "tp"),
            P("tp"),
            P("tp"),
            P("tp"),
            P("kv", "tp"),
            P("tp"),
            P("tp", "kv"),
            P("kv", None, "tp", None, None),
            P("kv", None, "tp"),
            P("kv", None, "tp"),
            P("kv", None, "tp"),
            P("kv"),
        ),
        out_specs=(
            P("tp", "kv"),
            P("kv", None, "tp", None, None),
            P("kv", None, "tp"),
            P("kv", None, "tp"),
            P("kv", None, "tp"),
        ),
        check_vma=False,
    )
```

time: 48.4 us -> 39.5 us (0.82)
  Pallas kernels: 46 us -> 38.7 us
  local copies, waits for them, and re-layouts: 1.4 us -> 0 us
    pallas_call x3 -> x2, Pallas kernels: 46 us -> 38.7 us  [the longest x1 33.9 us: per_device(): pl.pallas_call(functools.partial(mixer_kernel, nz, ny, nt, own, local * k...]
    unnamed x1 -> x0, local copies, waits for them, and re-layouts: 1.4 us -> none
where the time goes in v1:
time: 39.5 us; the launch traced here: 39.4 us
  Pallas kernels  38.7 us (98%)
  between operations  0.65 us (2%)
    pallas_call x1, Pallas kernels, per_device(): pl.pallas_call(functools.partial(mixer_kernel, nz, ny, nt, own, local * k...  33.9 us
    pallas_call x1, Pallas kernels, per_device(): pl.pallas_call(emit_kernel, out_shape=tuple((shape(dims, kind) for dims,...  4.79 us

profile of v1, /device:TPU:0, one launch (start us, length us, event | category | flops | bytes accessed | tf_op | source)
XLA Modules:
  0.0 39.4 jit_solution(13023804008194108215)
XLA Ops:
  0.6 33.9 %shard_map.236 = (bf16[40,512]{1,0:T(8,128)(2,1)S(1)}, f32[4,6,16,64,128]{4,3,2,1,0:T(8,128)S(1)}, bf16[4,8,1024]{2,1,0:T(8,128)(2,1)S(1)}, bf16[4,8,256]{2,1,0:T(8,128)(2,1)S(1)}, bf16[4,8,256]{2,1,0:T(8,128)(2,1)S(1)}) custom-call(bf16[160,512]{1,0:T(8,128)(2,1)} %tokens_h.1, f32[1,512]{1,0:T(1,128)} %bitcast.10, bf16[512,1024]{1,0:T(8,128)(2,1)} %in_h.1, ...), custom_call_target="tpu_custom_call" | custom-call | tf_op jit(solution)/shard_map/pallas_call | solution.py:524
  34.6 4.8 %shard_map.237 = (bf16[40,512]{1,0:T(8,128)(2,1)}, f32[4,6,16,64,128]{4,3,2,1,0:T(8,128)}, bf16[4,8,1024]{2,1,0:T(8,128)(2,1)}, bf16[4,8,256]{2,1,0:T(8,128)(2,1)}, bf16[4,8,256]{2,1,0:T(8,128)(2,1)}) custom-call(bf16[40,512]{1,0:T(8,128)(2,1)S(1)} %get-tuple-element.10.mix, f32[4,6,16,64,128]{4,3,2,1,0:T(8,128)S(1)} %get-tuple-element.11.states, ...), custom_call_target="tpu_custom_call" | custom-call | tf_op jit(solution)/shard_map/pallas_call | solution.py:570
